TPU v7x, 32 devices: a whole 2x2x4 slice. The times are simulated.
32 devices in a mesh: fs: 4 (over z), rep: 4 (over y, x), tp: 2 (over core).
Axes of the slice: x: 2, y: 2, z: 4, core: 2. Of those that a mesh axis runs over, the one named last changes fastest.
Arguments:
- query_input: bfloat16 [16384, 4096], P(('fs', 'rep')), may hold values from -6 to 6
- query_cotangent: bfloat16 [16384, 1024], P(('fs', 'rep'), 'tp'), may hold values from -0.046875 to 0.046875
- branch_output: bfloat16 [16384, 2048], P(('fs', 'rep')), may hold values from -6 to 6
- layer_cotangent: bfloat16 [16384, 4096], P(('fs', 'rep'), 'tp'), may hold values from -0.046875 to 0.046875
- query_weight: float32 [4096, 1024], P(('rep', 'fs'), 'tp'), may hold values from -0.09375 to 0.09375
- output_weight: float32 [2048, 4096], P(('rep', 'fs'), 'tp'), may hold values from -0.125 to 0.125
- query_basis: bfloat16 [4096, 512], P(('rep', 'fs')), may hold values from -0.09375 to 0.09375
- output_basis: bfloat16 [2048, 512], P(('rep', 'fs')), may hold values from -0.125 to 0.125
- query_first: float32 [512, 1024], P(('rep', 'fs'), 'tp'), may hold values from -20 to 20
- query_second: float32 [512, 1024], P(('rep', 'fs'), 'tp'), may hold values from 0.25 to 2
- output_first: float32 [512, 4096], P(('rep', 'fs'), 'tp'), may hold values from -20 to 20
- output_second: float32 [512, 4096], P(('rep', 'fs'), 'tp'), may hold values from 0.25 to 2
Outputs:
- query_update: float32 [4096, 1024], P(('rep', 'fs'), 'tp')
- output_update: float32 [2048, 4096], P(('rep', 'fs'), 'tp')
- query_first_next: float32 [512, 1024], P(('rep', 'fs'), 'tp')
- query_second_next: float32 [512, 1024], P(('rep', 'fs'), 'tp')
- output_first_next: float32 [512, 4096], P(('rep', 'fs'), 'tp')
- output_second_next: float32 [512, 4096], P(('rep', 'fs'), 'tp')
- query_copy: bfloat16 [4096, 1024], P('rep', 'tp')
- output_copy: bfloat16 [2048, 4096], P('rep', 'tp')
All inputs are finite; a program needn't handle non-finite values.
Results may differ from a plain program's by a relative error of at most 0.0055.
Values may be sent and summed in bfloat16 or wider, within the bound.
A program may use at most 128 MiB of HBM per device.

v0:
```python
import jax
import jax.numpy as jnp
from jax import lax
from jax.sharding import PartitionSpec as P

D = 4096
QKW = 1024
R = 512
beta_first = 0.6
beta_second = 0.8
step_rate = 0.01
small_eps = 1e-06


def split_parts(values):
    upper = values.astype(jnp.bfloat16)
    lower = (values - upper.astype(jnp.float32)).astype(jnp.bfloat16)
    return (upper, lower)


def split_rows(inner, cotangent):
    upper, lower = split_parts(inner)
    dims = (((0,), (0,)), ((), ()))
    return lax.dot_general(
        upper, cotangent, dims, preferred_element_type=jnp.float32
    ) + lax.dot_general(lower, cotangent, dims, preferred_element_type=jnp.float32)


def moments(first, second, projected):
    first_next = beta_first * first + (1.0 - beta_first) * projected
    second_next = beta_second * second + (1.0 - beta_second) * projected * projected
    return (first_next, second_next, first_next / jnp.sqrt(second_next))


def body(
    query_input,
    query_cotangent,
    branch_output,
    layer_cotangent,
    query_weight,
    output_weight,
    query_basis,
    output_basis,
    query_first,
    query_second,
    output_first,
    output_second,
):
    query_whole, output_whole = (
        lax.all_gather(query_basis, ("rep", "fs"), axis=0, tiled=True),
        lax.all_gather(output_basis, ("rep", "fs"), axis=0, tiled=True),
    )
    query_inner = jnp.dot(query_input, query_whole, preferred_element_type=jnp.float32)
    output_inner = jnp.dot(branch_output, output_whole, preferred_element_type=jnp.float32)
    projected_q = lax.psum_scatter(
        split_rows(query_inner, query_cotangent), ("rep", "fs"), scatter_dimension=0, tiled=True
    )
    projected_o = lax.psum_scatter(
        split_rows(output_inner, layer_cotangent), ("rep", "fs"), scatter_dimension=0, tiled=True
    )
    first_q, second_q, normed_q = moments(query_first, query_second, projected_q)
    first_o, second_o, normed_o = moments(output_first, output_second, projected_o)
    totals = lax.psum(
        (jnp.sum(normed_q * normed_q), jnp.sum(normed_o * normed_o)), ("fs", "rep", "tp")
    )
    scale_q = lax.rsqrt(totals[0] / (R * QKW) + small_eps)
    scale_o = lax.rsqrt(totals[1] / (R * D) + small_eps)
    summed_q = jnp.dot(
        query_basis,
        lax.all_gather(normed_q.astype(jnp.bfloat16), ("rep", "fs"), axis=0, tiled=True),
        preferred_element_type=jnp.float32,
    )
    summed_o = jnp.dot(
        output_basis,
        lax.all_gather(normed_o.astype(jnp.bfloat16), ("rep", "fs"), axis=0, tiled=True),
        preferred_element_type=jnp.float32,
    )
    update_q = scale_q * summed_q
    update_o = scale_o * summed_o
    query_copy, output_copy = (
        lax.all_gather(
            (query_weight - step_rate * update_q).astype(jnp.bfloat16), "fs", axis=0, tiled=True
        ),
        lax.all_gather(
            (output_weight - step_rate * update_o).astype(jnp.bfloat16), "fs", axis=0, tiled=True
        ),
    )
    return (update_q, update_o, first_q, second_q, first_o, second_o, query_copy, output_copy)


def solution(mesh):
    in_specs = (
        P(("fs", "rep"), None),
        P(("fs", "rep"), "tp"),
        P(("fs", "rep"), None),
        P(("fs", "rep"), "tp"),
        P(("rep", "fs"), "tp"),
        P(("rep", "fs"), "tp"),
        P(("rep", "fs"), None),
        P(("rep", "fs"), None),
        P(("rep", "fs"), "tp"),
        P(("rep", "fs"), "tp"),
        P(("rep", "fs"), "tp"),
        P(("rep", "fs"), "tp"),
    )
    out_specs = (
        P(("rep", "fs"), "tp"),
        P(("rep", "fs"), "tp"),
        P(("rep", "fs"), "tp"),
        P(("rep", "fs"), "tp"),
        P(("rep", "fs"), "tp"),
        P(("rep", "fs"), "tp"),
        P("rep", "tp"),
        P("rep", "tp"),
    )
    return jax.shard_map(body, mesh=mesh, in_specs=in_specs, out_specs=out_specs, check_vma=False)
```

profile of v0, /device:TPU:0, one launch (start us, length us, event | category | flops | bytes accessed | tf_op | source)
XLA Modules:
  0.0 505.3 jit_solution(10517695907345015072)
XLA Ops:
  7.2 0.7 all-gather.8.cloned.1.call-update
  8.0 0.7 all-gather.6.cloned.1.call-update
  8.7 65.3 %all-gather.8.cloned.1.call-done = bf16[2048,512]{1,0:T(8,128)(2,1)} async-done(((bf16[128,512]{1,0:T(8,128)(2,1)}), bf16[2048,512]{1,0:T(8,128)(2,1)}) %all-gather.8.cloned.1.call-update) | async-done | bytes 2097168 | tf_op jit(solution)/shard_map/all_gather | solution.py:51
  74.0 5.3 %fusion.15 = f32[1024,512]{1,0:T(8,128)S(1)} fusion(bf16[1024,2048]{1,0:T(8,128)(2,1)} %param.14, bf16[2048,512]{1,0:T(8,128)(2,1)} %all-gather.8.cloned.1.call-done), kind=kOutput, calls=%fused_computation.29 | convolution fusion | flops 2147483648 | bytes 8388608 | tf_op jit(solution)/shard_map/dot_general | solution.py:54
  79.4 2.4 fusion.3
  81.7 4.4 convolution_add_fusion
  86.2 0.0 reduce-scatter.3.cloned.1.call-start
  86.2 65.0 %all-gather.6.cloned.1.call-done = bf16[4096,512]{1,0:T(8,128)(2,1)} async-done(((bf16[256,512]{1,0:T(8,128)(2,1)}), bf16[4096,512]{1,0:T(8,128)(2,1)}) %all-gather.6.cloned.1.call-update) | async-done | bytes 4194320 | tf_op jit(solution)/shard_map/all_gather | solution.py:50
  151.2 8.1 %fusion.14 = f32[1024,512]{1,0:T(8,128)S(1)} fusion(bf16[1024,4096]{1,0:T(8,128)(2,1)} %param.12, bf16[4096,512]{1,0:T(8,128)(2,1)} %all-gather.6.cloned.1.call-done), kind=kOutput, calls=%fused_computation.28 | convolution fusion | flops 4294967296 | bytes 14680064 | tf_op jit(solution)/shard_map/dot_general | solution.py:53
  159.3 0.7 fusion.6
  160.1 1.7 convolution_add_fusion.1
  161.9 0.0 all-gather.10.cloned.1.call-start
  161.9 87.6 %reduce-scatter.5.cloned.1.call-done = f32[32,2048]{1,0:T(8,128)} async-done(((f32[512,2048]{1,0:T(8,128)}), f32[32,2048]{1,0:T(8,128)}) %reduce-scatter.5.cloned.1.call-update) | async-done | bytes 262160 | tf_op jit(solution)/shard_map/reduce_scatter | solution.py:58
  249.6 1.7 fusion.9
  251.3 0.0 all-gather.12.cloned.1.call-start
  251.3 0.2 copy.20
  251.5 79.1 %reduce-scatter.3.cloned.1.call-done = f32[32,512]{1,0:T(8,128)} async-done(((f32[512,512]{1,0:T(8,128)}), f32[32,512]{1,0:T(8,128)}) %reduce-scatter.3.cloned.1.call-update) | async-done | bytes 65552 | tf_op jit(solution)/shard_map/reduce_scatter | solution.py:55
  330.6 1.5 multiply_reduce_fusion.1
  332.1 0.6 copy-done.7
  332.8 43.2 %all_gather.19 = bf16[512,512]{1,0:T(8,128)(2,1)S(1)} all-gather(bf16[32,512]{1,0:T(8,128)(2,1)S(1)} %fusion.11), channel_id=1, replica_groups=mesh['fs'=4,'rep'=4,'tp'=2] {'rep','fs'}, dimensions={0}, use_global_device_ids=true | all-gather | bytes 557056 | tf_op jit(solution)/shard_map/all_gather | solution.py:70
  376.0 0.7 multiply_reduce_fusion
  376.7 37.8 %all-reduce = (f32[]{:T(128)}, f32[]{:T(128)}) all-reduce(f32[]{:T(128)} %get-tuple-element.21, f32[]{:T(128)} %multiply_reduce_fusion), channel_id=1, replica_groups=mesh['fs'=4,'rep'=4,'tp'=2] {'fs','rep','tp'}, use_global_device_ids=true, to_apply=%region_2.0 | all-reduce | flops 2 | bytes 16 | tf_op jit(solution)/shard_map/psum | solution.py:63
  415.2 1.2 subtract_convert_fusion.5
  416.4 0.0 all-gather.14.cloned.1.call-start
  416.5 1.6 copy.21
  418.8 3.1 subtract_convert_fusion.4
  421.9 2.0 copy.22
  424.0 23.8 %all-gather.12.cloned.1.call-done = bf16[1024,512]{0,1:T(8,128)(2,1)} async-done(((bf16[256,512]{0,1:T(8,128)(2,1)}), bf16[1024,512]{0,1:T(8,128)(2,1)}) %all-gather.12.cloned.1.call-update) | async-done | bytes 1048592 | tf_op jit(solution)/shard_map/all_gather | solution.py:81
  447.8 2.3 copy.24
  450.1 1.3 copy.23
  451.4 43.1 %all-gather.14.cloned.1.call-done = bf16[512,2048]{0,1:T(8,128)(2,1)} async-done(((bf16[128,2048]{0,1:T(8,128)(2,1)}), bf16[512,2048]{0,1:T(8,128)(2,1)}) %all-gather.14.cloned.1.call-update) | async-done | bytes 2097168 | tf_op jit(solution)/shard_map/all_gather | solution.py:84
  494.5 3.9 copy.25
  (35 shorter events, 0.3 us)
Async XLA Ops:
  7.2 152.2 %copy-start = (bf16[1024,512]{1,0:T(8,128)(2,1)S(1)}, bf16[1024,512]{1,0:T(8,128)(2,1)}, u32[]{:S(2)}) copy-start(bf16[1024,512]{1,0:T(8,128)(2,1)} %param.13) | copy-start | bytes 3145732
  7.2 66.8 %all-gather.8.cloned.1.call-start = ((), (), s32[]{:S(2)}) async-start(), calls=%async_computation.4 | async-start | bytes 2228224 | tf_op jit(solution)/shard_map/all_gather | solution.py:51
  7.9 143.3 %all-gather.6.cloned.1.call-start = ((), (), s32[]{:S(2)}) async-start(), calls=%async_computation.2 | async-start | bytes 4456448 | tf_op jit(solution)/shard_map/all_gather | solution.py:50
  8.7 240.9 %reduce-scatter.5.cloned.1.call-start = ((), (), s32[]{:S(2)}) async-start(), calls=%async_computation.5 | async-start | bytes 4456448 | tf_op jit(solution)/shard_map/reduce_scatter | solution.py:58
  74.0 5.3 %copy-start.1 = (bf16[1024,2048]{1,0:T(8,128)(2,1)S(1)}, bf16[1024,2048]{1,0:T(8,128)(2,1)}, u32[]{:S(2)}) copy-start(bf16[1024,2048]{1,0:T(8,128)(2,1)} %param.15) | copy-start | bytes 12582916
  86.2 244.5 %reduce-scatter.3.cloned.1.call-start = ((), (), s32[]{:S(2)}) async-start(), calls=%async_computation.3 | async-start | bytes 1114112 | tf_op jit(solution)/shard_map/reduce_scatter | solution.py:55
  160.1 89.5 %copy-start.9 = (f32[32,2048]{1,0:T(8,128)S(1)}, f32[32,2048]{1,0:T(8,128)}, u32[]{:S(2)}) copy-start(f32[32,2048]{1,0:T(8,128)} %param.23) | copy-start | bytes 786436
  160.1 89.5 %copy-start.10 = (f32[32,2048]{1,0:T(8,128)S(1)}, f32[32,2048]{1,0:T(8,128)}, u32[]{:S(2)}) copy-start(f32[32,2048]{1,0:T(8,128)} %param.22) | copy-start | bytes 786436
  161.8 89.5 %copy-start.6 = (f32[256,512]{1,0:T(8,128)S(1)}, f32[256,512]{1,0:T(8,128)}, u32[]{:S(2)}) copy-start(f32[256,512]{1,0:T(8,128)} %param.16) | copy-start | bytes 1572868
  161.8 168.8 %copy-start.11 = (f32[32,512]{1,0:T(8,128)S(1)}, f32[32,512]{1,0:T(8,128)}, u32[]{:S(2)}) copy-start(f32[32,512]{1,0:T(8,128)} %param.21) | copy-start | bytes 196612
  161.8 168.8 %copy-start.12 = (f32[32,512]{1,0:T(8,128)S(1)}, f32[32,512]{1,0:T(8,128)}, u32[]{:S(2)}) copy-start(f32[32,512]{1,0:T(8,128)} %param.20) | copy-start | bytes 196612
  161.8 253.3 %copy-start.2 = (bf16[256,512]{1,0:T(8,128)(2,1)S(1)}, bf16[256,512]{1,0:T(8,128)(2,1)}, u32[]{:S(2)}) copy-start(bf16[256,512]{1,0:T(8,128)(2,1)} %param.18) | copy-start | bytes 786436
  161.9 256.9 %all-gather.10.cloned.1.call-start = ((), (), s32[]{:S(2)}) async-start(), calls=%async_computation.6 | async-start | bytes 2228224 | tf_op jit(solution)/shard_map/all_gather | solution.py:75
  251.3 165.2 %copy-start.3 = (f32[32,2048]{1,0:T(8,128)}, f32[32,2048]{1,0:T(8,128)S(1)}, u32[]{:S(2)}) copy-start(f32[32,2048]{1,0:T(8,128)S(1)} %get-tuple-element.19) | copy-start | bytes 786436
  251.3 165.2 %copy-start.4 = (f32[32,2048]{1,0:T(8,128)}, f32[32,2048]{1,0:T(8,128)S(1)}, u32[]{:S(2)}) copy-start(f32[32,2048]{1,0:T(8,128)S(1)} %get-tuple-element.20) | copy-start | bytes 786436
  251.3 196.5 %all-gather.12.cloned.1.call-start = ((), (), s32[]{:S(2)}) async-start(), calls=%async_computation.7 | async-start | bytes 1310720 | tf_op jit(solution)/shard_map/all_gather | solution.py:81
  332.1 0.6 copy-start.7
  332.1 0.6 copy-start.8
  415.2 3.6 copy-start.5
  416.4 78.1 %all-gather.14.cloned.1.call-start = ((), (), s32[]{:S(2)}) async-start(), calls=%async_computation.8 | async-start | bytes 2621440 | tf_op jit(solution)/shard_map/all_gather | solution.py:84
Sparse Core Ops, SparseCore 0:
  10.8 63.1 all-gather.7
  76.8 74.3 all-gather.5
  153.5 96.0 reduce-scatter.4
  252.2 78.3 reduce-scatter.2
  333.9 58.0 all-gather.9
  416.6 31.1 all-gather.11
  449.9 44.5 all-gather.13
where the time goes:
time: 506 us; the launch traced here: 505 us
  waiting for transfers between devices  365 us (72%)
  blocking collectives  81 us (16%)
  matrix products  27.1 us (5%)
  between operations  15.7 us (3%)
  local copies, waits for them, and re-layouts  12 us (2%)
    reduce_scatter x1, waiting for transfers between devices, body(): lax.psum_scatter(split_rows(output_inner, layer_cotangent), ('rep', 'fs')...  87.6 us
    reduce_scatter x1, waiting for transfers between devices, body(): lax.psum_scatter(split_rows(query_inner, query_cotangent), ('rep', 'fs'),...  79.1 us
    all_gather x1, waiting for transfers between devices, body(): lax.all_gather(output_basis, ('rep', 'fs'), axis=0, tiled=True)  65.3 us
    all_gather x1, waiting for transfers between devices, body(): lax.all_gather(query_basis, ('rep', 'fs'), axis=0, tiled=True)  65 us
    all_gather x1, blocking collectives, body(): lax.all_gather(normed_q.astype(jnp.bfloat16), ('rep', 'fs'), axis=0, tile...  43.2 us
    all_gather x1, waiting for transfers between devices, body(): lax.all_gather((output_weight - step_rate * update_o).astype(jnp.bfloat16...  43.1 us
    psum x1, blocking collectives, body(): lax.psum((jnp.sum(normed_q * normed_q), jnp.sum(normed_o * normed_o)), ('...  37.8 us
    all_gather x1, waiting for transfers between devices, body(): lax.all_gather((query_weight - step_rate * update_q).astype(jnp.bfloat16)...  23.8 us
  transfers between devices with their start and end apart: 7, of which 6 were waited for; matrix products, arithmetic and copies ran while one was open for 8% of the time, Pallas kernels for 0%

commit v1 on v0

--- a/solution.py
+++ b/solution.py
@@ -46,6 +46,12 @@
     output_first,
     output_second,
 ):
+
+    def _put_types(vec, bus_axis, mesh_name):
+        for dd in (bus_axis, mesh_name):
+            vec = lax.psum(vec, dd)
+        return vec
+
     query_whole, output_whole = (
         lax.all_gather(query_basis, ("rep", "fs"), axis=0, tiled=True),
         lax.all_gather(output_basis, ("rep", "fs"), axis=0, tiled=True),
@@ -60,8 +66,8 @@
     )
     first_q, second_q, normed_q = moments(query_first, query_second, projected_q)
     first_o, second_o, normed_o = moments(output_first, output_second, projected_o)
-    totals = lax.psum(
-        (jnp.sum(normed_q * normed_q), jnp.sum(normed_o * normed_o)), ("fs", "rep", "tp")
+    totals = _put_types(
+        (jnp.sum(normed_q * normed_q), jnp.sum(normed_o * normed_o)), ("rep", "tp"), "fs"
     )
     scale_q = lax.rsqrt(totals[0] / (R * QKW) + small_eps)
     scale_o = lax.rsqrt(totals[1] / (R * D) + small_eps)

time: 506 us -> 488 us (0.964)
  blocking collectives: 81 us -> 65.7 us
    psum x1 -> x2, blocking collectives: 37.8 us -> 22.5 us  [_put_types(): vec = lax.psum(vec, dd)]
where the time goes in v1:
time: 488 us; the launch traced here: 487 us
  waiting for transfers between devices  363 us (74%)
  blocking collectives  65.7 us (13%)
  matrix products  27.1 us (6%)
  between operations  15.7 us (3%)
  local copies, waits for them, and re-layouts  12 us (2%)
    reduce_scatter x1, waiting for transfers between devices, body(): lax.psum_scatter(split_rows(output_inner, layer_cotangent), ('rep', 'fs')...  87.6 us
    reduce_scatter x1, waiting for transfers between devices, body(): lax.psum_scatter(split_rows(query_inner, query_cotangent), ('rep', 'fs'),...  79.1 us
    all_gather x1, waiting for transfers between devices, body(): lax.all_gather(output_basis, ('rep', 'fs'), axis=0, tiled=True)  65.3 us
    all_gather x1, waiting for transfers between devices, body(): lax.all_gather(query_basis, ('rep', 'fs'), axis=0, tiled=True)  65 us
    all_gather x1, blocking collectives, body(): lax.all_gather(normed_q.astype(jnp.bfloat16), ('rep', 'fs'), axis=0, tile...  43.2 us
    all_gather x1, waiting for transfers between devices, body(): lax.all_gather((output_weight - step_rate * update_o).astype(jnp.bfloat16...  43.1 us
    psum x2, blocking collectives, _put_types(): vec = lax.psum(vec, dd)  22.5 us
    all_gather x1, waiting for transfers between devices, body(): lax.all_gather((query_weight - step_rate * update_q).astype(jnp.bfloat16)...  20.9 us
  transfers between devices with their start and end apart: 7, of which 6 were waited for; matrix products, arithmetic and copies ran while one was open for 8% of the time, Pallas kernels for 0%

profile of v1, /device:TPU:0, one launch (start us, length us, event | category | flops | bytes accessed | tf_op | source)
XLA Modules:
  0.0 487.2 jit_solution(12631001307843496341)
XLA Ops:
  7.2 0.7 all-gather.8.cloned.1.call-update
  8.0 0.7 all-gather.6.cloned.1.call-update
  8.7 65.3 %all-gather.8.cloned.1.call-done = bf16[2048,512]{1,0:T(8,128)(2,1)} async-done(((bf16[128,512]{1,0:T(8,128)(2,1)}), bf16[2048,512]{1,0:T(8,128)(2,1)}) %all-gather.8.cloned.1.call-update) | async-done | bytes 2097168 | tf_op jit(solution)/shard_map/all_gather | solution.py:57
  74.0 5.3 %fusion.15 = f32[1024,512]{1,0:T(8,128)S(1)} fusion(bf16[1024,2048]{1,0:T(8,128)(2,1)} %param.14, bf16[2048,512]{1,0:T(8,128)(2,1)} %all-gather.8.cloned.1.call-done), kind=kOutput, calls=%fused_computation.29 | convolution fusion | flops 2147483648 | bytes 8388608 | tf_op jit(solution)/shard_map/dot_general | solution.py:60
  79.4 2.4 fusion.3
  81.7 4.4 convolution_add_fusion
  86.2 0.0 reduce-scatter.3.cloned.1.call-start
  86.2 65.0 %all-gather.6.cloned.1.call-done = bf16[4096,512]{1,0:T(8,128)(2,1)} async-done(((bf16[256,512]{1,0:T(8,128)(2,1)}), bf16[4096,512]{1,0:T(8,128)(2,1)}) %all-gather.6.cloned.1.call-update) | async-done | bytes 4194320 | tf_op jit(solution)/shard_map/all_gather | solution.py:56
  151.2 8.1 %fusion.14 = f32[1024,512]{1,0:T(8,128)S(1)} fusion(bf16[1024,4096]{1,0:T(8,128)(2,1)} %param.12, bf16[4096,512]{1,0:T(8,128)(2,1)} %all-gather.6.cloned.1.call-done), kind=kOutput, calls=%fused_computation.28 | convolution fusion | flops 4294967296 | bytes 14680064 | tf_op jit(solution)/shard_map/dot_general | solution.py:59
  159.3 0.7 fusion.6
  160.1 1.7 convolution_add_fusion.1
  161.9 0.0 all-gather.10.cloned.1.call-start
  161.9 87.6 %reduce-scatter.5.cloned.1.call-done = f32[32,2048]{1,0:T(8,128)} async-done(((f32[512,2048]{1,0:T(8,128)}), f32[32,2048]{1,0:T(8,128)}) %reduce-scatter.5.cloned.1.call-update) | async-done | bytes 262160 | tf_op jit(solution)/shard_map/reduce_scatter | solution.py:64
  249.6 1.7 fusion.9
  251.3 0.0 all-gather.12.cloned.1.call-start
  251.3 0.2 copy.20
  251.5 79.1 %reduce-scatter.3.cloned.1.call-done = f32[32,512]{1,0:T(8,128)} async-done(((f32[512,512]{1,0:T(8,128)}), f32[32,512]{1,0:T(8,128)}) %reduce-scatter.3.cloned.1.call-update) | async-done | bytes 65552 | tf_op jit(solution)/shard_map/reduce_scatter | solution.py:61
  330.6 1.5 multiply_reduce_fusion.1
  332.1 0.6 copy-done.7
  332.8 43.2 %all_gather.19 = bf16[512,512]{1,0:T(8,128)(2,1)S(1)} all-gather(bf16[32,512]{1,0:T(8,128)(2,1)S(1)} %fusion.11), channel_id=1, replica_groups=mesh['fs'=4,'rep'=4,'tp'=2] {'rep','fs'}, dimensions={0}, use_global_device_ids=true | all-gather | bytes 557056 | tf_op jit(solution)/shard_map/all_gather | solution.py:76
  376.0 0.7 multiply_reduce_fusion
  376.7 13.5 %all-reduce = (f32[]{:T(128)}, f32[]{:T(128)}) all-reduce(f32[]{:T(128)} %get-tuple-element.23, f32[]{:T(128)} %multiply_reduce_fusion), channel_id=1, replica_groups=mesh['fs'=4,'rep'=4,'tp'=2] {'rep','tp'}, use_global_device_ids=true, to_apply=%region_2.0 | all-reduce | flops 2 | bytes 16 | tf_op jit(solution)/shard_map/psum | solution.py:52
  390.2 9.0 %all-reduce.1 = (f32[]{:T(128)}, f32[]{:T(128)}) all-reduce(f32[]{:T(128)} %get-tuple-element.16, f32[]{:T(128)} %get-tuple-element.17), channel_id=1, replica_groups=mesh['fs'=4,'rep'=4,'tp'=2] {'fs'}, use_global_device_ids=true, to_apply=%region_3.0 | all-reduce | flops 2 | bytes 16 | tf_op jit(solution)/shard_map/psum | solution.py:52
  399.9 1.2 subtract_convert_fusion.5
  401.2 1.6 copy.21
  403.5 3.1 subtract_convert_fusion.4
  406.7 2.1 copy.22
  408.7 20.9 %all-gather.12.cloned.1.call-done = bf16[1024,512]{0,1:T(8,128)(2,1)} async-done(((bf16[256,512]{0,1:T(8,128)(2,1)}), bf16[1024,512]{0,1:T(8,128)(2,1)}) %all-gather.12.cloned.1.call-update) | async-done | bytes 1048592 | tf_op jit(solution)/shard_map/all_gather | solution.py:87
  429.7 2.3 copy.24
  431.9 1.3 copy.23
  433.3 43.1 %all-gather.14.cloned.1.call-done = bf16[512,2048]{0,1:T(8,128)(2,1)} async-done(((bf16[128,2048]{0,1:T(8,128)(2,1)}), bf16[512,2048]{0,1:T(8,128)(2,1)}) %all-gather.14.cloned.1.call-update) | async-done | bytes 2097168 | tf_op jit(solution)/shard_map/all_gather | solution.py:90
  476.4 3.9 copy.25
  (36 shorter events, 0.4 us)
Async XLA Ops:
  7.2 152.2 %copy-start = (bf16[1024,512]{1,0:T(8,128)(2,1)S(1)}, bf16[1024,512]{1,0:T(8,128)(2,1)}, u32[]{:S(2)}) copy-start(bf16[1024,512]{1,0:T(8,128)(2,1)} %param.13) | copy-start | bytes 3145732
  7.2 66.8 %all-gather.8.cloned.1.call-start = ((), (), s32[]{:S(2)}) async-start(), calls=%async_computation.4 | async-start | bytes 2228224 | tf_op jit(solution)/shard_map/all_gather | solution.py:57
  7.9 143.3 %all-gather.6.cloned.1.call-start = ((), (), s32[]{:S(2)}) async-start(), calls=%async_computation.2 | async-start | bytes 4456448 | tf_op jit(solution)/shard_map/all_gather | solution.py:56
  8.7 240.9 %reduce-scatter.5.cloned.1.call-start = ((), (), s32[]{:S(2)}) async-start(), calls=%async_computation.5 | async-start | bytes 4456448 | tf_op jit(solution)/shard_map/reduce_scatter | solution.py:64
  74.0 5.3 %copy-start.1 = (bf16[1024,2048]{1,0:T(8,128)(2,1)S(1)}, bf16[1024,2048]{1,0:T(8,128)(2,1)}, u32[]{:S(2)}) copy-start(bf16[1024,2048]{1,0:T(8,128)(2,1)} %param.15) | copy-start | bytes 12582916
  86.2 244.5 %reduce-scatter.3.cloned.1.call-start = ((), (), s32[]{:S(2)}) async-start(), calls=%async_computation.3 | async-start | bytes 1114112 | tf_op jit(solution)/shard_map/reduce_scatter | solution.py:61
  160.1 89.5 %copy-start.9 = (f32[32,2048]{1,0:T(8,128)S(1)}, f32[32,2048]{1,0:T(8,128)}, u32[]{:S(2)}) copy-start(f32[32,2048]{1,0:T(8,128)} %param.23) | copy-start | bytes 786436
  160.1 89.5 %copy-start.10 = (f32[32,2048]{1,0:T(8,128)S(1)}, f32[32,2048]{1,0:T(8,128)}, u32[]{:S(2)}) copy-start(f32[32,2048]{1,0:T(8,128)} %param.22) | copy-start | bytes 786436
  161.8 89.5 %copy-start.6 = (f32[256,512]{1,0:T(8,128)S(1)}, f32[256,512]{1,0:T(8,128)}, u32[]{:S(2)}) copy-start(f32[256,512]{1,0:T(8,128)} %param.16) | copy-start | bytes 1572868
  161.8 168.8 %copy-start.11 = (f32[32,512]{1,0:T(8,128)S(1)}, f32[32,512]{1,0:T(8,128)}, u32[]{:S(2)}) copy-start(f32[32,512]{1,0:T(8,128)} %param.21) | copy-start | bytes 196612
  161.8 168.8 %copy-start.12 = (f32[32,512]{1,0:T(8,128)S(1)}, f32[32,512]{1,0:T(8,128)}, u32[]{:S(2)}) copy-start(f32[32,512]{1,0:T(8,128)} %param.20) | copy-start | bytes 196612
  161.8 238.1 %copy-start.2 = (bf16[256,512]{1,0:T(8,128)(2,1)S(1)}, bf16[256,512]{1,0:T(8,128)(2,1)}, u32[]{:S(2)}) copy-start(bf16[256,512]{1,0:T(8,128)(2,1)} %param.18) | copy-start | bytes 786436
  161.9 241.6 %all-gather.10.cloned.1.call-start = ((), (), s32[]{:S(2)}) async-start(), calls=%async_computation.6 | async-start | bytes 2228224 | tf_op jit(solution)/shard_map/all_gather | solution.py:81
  251.3 149.9 %copy-start.3 = (f32[32,2048]{1,0:T(8,128)}, f32[32,2048]{1,0:T(8,128)S(1)}, u32[]{:S(2)}) copy-start(f32[32,2048]{1,0:T(8,128)S(1)} %get-tuple-element.21) | copy-start | bytes 786436
  251.3 149.9 %copy-start.4 = (f32[32,2048]{1,0:T(8,128)}, f32[32,2048]{1,0:T(8,128)S(1)}, u32[]{:S(2)}) copy-start(f32[32,2048]{1,0:T(8,128)S(1)} %get-tuple-element.22) | copy-start | bytes 786436
  251.3 178.4 %all-gather.12.cloned.1.call-start = ((), (), s32[]{:S(2)}) async-start(), calls=%async_computation.7 | async-start | bytes 1310720 | tf_op jit(solution)/shard_map/all_gather | solution.py:87
  332.1 0.6 copy-start.7
  332.1 0.6 copy-start.8
  399.9 3.6 copy-start.5
  401.2 75.2 %all-gather.14.cloned.1.call-start = ((), (), s32[]{:S(2)}) async-start(), calls=%async_computation.8 | async-start | bytes 2621440 | tf_op jit(solution)/shard_map/all_gather | solution.py:90
Sparse Core Ops, SparseCore 0:
  10.8 63.1 all-gather.7
  76.8 74.3 all-gather.5
  153.5 96.0 reduce-scatter.4
  252.2 78.3 reduce-scatter.2
  333.9 57.8 all-gather.9
  401.3 28.3 all-gather.11
  431.8 44.5 all-gather.13
